TPU v7x, 768 devices: a whole 4x8x12 slice. The times are simulated.
768 devices in a mesh: fs: 24 (over z, core), tp: 32 (over y, x).
Axes of the slice: x: 4, y: 8, z: 12, core: 2. Of those that a mesh axis runs over, the one named last changes fastest.
Arguments:
- inputs: bfloat16 [6144, 2016], P('fs'), may hold values from -6 to 6
- pre_act: bfloat16 [6144, 4032], P('fs', 'tp'), may hold values from -6 to 6
- cotangent: bfloat16 [6144, 2016], P('fs'), may hold values from -6 to 6
- w_up: bfloat16 [2016, 4032], P('fs', 'tp'), may hold values from -0.125 to 0.125
- w_down: bfloat16 [4032, 2016], P('tp', 'fs'), may hold values from -0.09375 to 0.09375
Outputs:
- grad_input: bfloat16 [6144, 2016], P('fs')
- grad_up: float32 [2016, 4032], P('fs', 'tp')
- grad_down: float32 [4032, 2016], P('tp', 'fs')
All inputs are finite; a program needn't handle non-finite values.
Results may differ from a plain program's by a relative error of at most 0.017.
Values may be sent and summed in bfloat16 or wider, within the bound.
A program may use at most 32 MiB of HBM per device.

v0:
```python
import jax
import jax.numpy as jnp
from jax import lax
from jax.sharding import Mesh
from jax.sharding import PartitionSpec as P

TP = ("tp_0", "tp_1")


def sent_to_all(value, axis):
    length = lax.axis_size(axis)
    return lax.all_to_all(
        jnp.broadcast_to(value[None], (length, *value.shape)), axis, 0, 0, tiled=True
    )


def joined_along(blocks, dim):
    shape = list(blocks.shape[1:])
    shape[dim] *= blocks.shape[0]
    return jnp.moveaxis(blocks, 0, dim).reshape(shape)


def collect(value, axis, dim):
    blocks = sent_to_all(value, axis)
    return joined_along(blocks, dim)


def split_up(value, dim, length):
    shape = value.shape
    blocks = value.reshape(*shape[:dim], length, shape[dim] // length, *shape[dim + 1 :])
    return jnp.moveaxis(blocks, dim, 0)


def sent_and_summed(value, axis, dim):
    length = lax.axis_size(axis)
    blocks = lax.all_to_all(split_up(value, dim, length), axis, 0, 0, tiled=True)
    return jnp.sum(blocks.astype(jnp.float32), axis=0)


def gathered_by_axis(value, axes, dim):
    for axis in reversed(axes):
        value = lax.all_gather(value, axis, axis=dim, tiled=True)
    return value


def on_device(inputs, pre_act, cotangent, w_up, w_down):
    positive = jnp.maximum(pre_act.astype(jnp.float32), 0.0)
    hidden = (positive * positive).astype(jnp.bfloat16)
    columns = cotangent
    hidden_grad = lax.dot_general(
        columns,
        collect(w_down, "fs", 1),
        (((1,), (1,)), ((), ())),
        preferred_element_type=jnp.float32,
    )
    pre_grad = (2.0 * positive * hidden_grad).astype(jnp.bfloat16)
    width = w_up.shape[1]
    columns = inputs
    joined = sent_and_summed(
        jnp.concatenate(
            [
                lax.dot_general(
                    columns, pre_grad, (((0,), (0,)), ((), ())), preferred_element_type=jnp.float32
                ),
                lax.dot_general(
                    cotangent, hidden, (((0,), (0,)), ((), ())), preferred_element_type=jnp.float32
                ),
            ],
            axis=1,
        ).astype(jnp.bfloat16),
        "fs",
        0,
    )
    grad_up = joined[:, :width]
    grad_down = joined[:, width:].T
    partial_sum = lax.dot_general(
        pre_grad,
        collect(w_up, "fs", 0),
        (((1,), (1,)), ((), ())),
        preferred_element_type=jnp.float32,
    ).astype(jnp.bfloat16)
    shares = sent_and_summed(partial_sum, TP, 0).astype(jnp.bfloat16)
    grad_input = gathered_by_axis(shares, TP, 0)
    return (grad_input, grad_up, grad_down)


def solution(mesh):
    split = Mesh(mesh.devices.reshape(mesh.shape["fs"], 8, 4), ("fs", "tp_0", "tp_1"))
    return jax.shard_map(
        on_device,
        mesh=split,
        in_specs=(P("fs", None), P("fs", TP), P("fs", None), P("fs", TP), P(TP, "fs")),
        out_specs=(P("fs", None), P("fs", TP), P(TP, "fs")),
        check_vma=False,
    )
```

profile of v0, /device:TPU:1, one launch (start us, length us, event | category | flops | bytes accessed | tf_op | source)
XLA Modules:
  0.0 157.9 jit_solution(16484042202934221718)
XLA Ops:
  0.7 0.9 broadcast_in_dim.4
  1.6 39.6 %all_to_all.20 = bf16[24,126,84]{1,2,0:T(8,128)(2,1)S(1)} all-to-all(bf16[24,126,84]{1,2,0:T(8,128)(2,1)S(1)} %broadcast_in_dim.4), channel_id=1, replica_groups=mesh['fs'=24,'tp_0'=8,'tp_1'=4] {'fs'}, dimensions={0} | all-to-all | bytes 1016064 | tf_op jit(solution)/shard_map/all_to_all | solution.py:12
  41.2 0.9 broadcast_in_dim.5
  42.0 6.1 %all-to-all-start.1 = ((bf16[24,84,126]{2,1,0:T(8,128)(2,1)}), bf16[24,84,126]{2,1,0:T(8,128)(2,1)S(1)}, u32[]{:S(2)}, u32[]{:S(2)}) async-start(bf16[24,84,126]{2,1,0:T(8,128)(2,1)} %broadcast_in_dim.5), calls=%async_computation.1 | async-start | bytes 1081344 | tf_op jit(solution)/shard_map/all_to_all | solution.py:12
  48.2 0.2 reshape.22
  48.3 0.5 fusion.2
  48.8 22.4 %all-to-all-done.1 = bf16[24,84,126]{2,1,0:T(8,128)(2,1)S(1)} async-done(((bf16[24,84,126]{2,1,0:T(8,128)(2,1)}), bf16[24,84,126]{2,1,0:T(8,128)(2,1)S(1)}, u32[]{:S(2)}, u32[]{:S(2)}) %all-to-all-start.1) | async-done | bytes 508064 | tf_op jit(solution)/shard_map/all_to_all | solution.py:12
  71.2 0.2 reshape.23
  71.4 0.4 convolution_convert_fusion
  71.8 1.4 copy.10
  73.3 9.7 %all-to-all-start.2 = ((bf16[32,8,2016]{2,1,0:T(8,128)(2,1)}), bf16[32,8,2016]{2,1,0:T(8,128)(2,1)S(1)}, u32[]{:S(2)}, u32[]{:S(2)}) async-start(bf16[32,8,2016]{2,1,0:T(8,128)(2,1)} %bitcast.1), calls=%async_computation.2 | async-start | bytes 2097152 | tf_op jit(solution)/shard_map/all_to_all | solution.py:36
  82.9 0.4 fusion.1
  83.5 2.4 %fusion = bf16[2016,126]{1,0:T(8,128)(2,1)} fusion(bf16[256,126]{1,0:T(8,128)(2,1)S(1)} %fusion.2, bf16[256,2016]{0,1:T(8,128)(2,1)} %param.5), kind=kOutput, calls=%fused_computation.3 | convolution fusion | flops 130310208 | bytes 1604736 | tf_op jit(solution)/shard_map/dot_general | solution.py:62
  86.0 1.2 concatenate.9
  87.1 1.5 pad_maximum_fusion
  88.6 19.3 %all-to-all-done.2 = bf16[32,8,2016]{2,1,0:T(8,128)(2,1)S(1)} async-done(((bf16[32,8,2016]{2,1,0:T(8,128)(2,1)}), bf16[32,8,2016]{2,1,0:T(8,128)(2,1)S(1)}, u32[]{:S(2)}, u32[]{:S(2)}) %all-to-all-start.2) | async-done | bytes 1032224 | tf_op jit(solution)/shard_map/all_to_all | solution.py:36
  107.8 9.5 %all-to-all-start.3 = ((bf16[24,84,252]{2,1,0:T(8,128)(2,1)}), bf16[24,84,252]{2,1,0:T(8,128)(2,1)S(1)}, u32[]{:S(2)}, u32[]{:S(2)}) async-start(bf16[24,84,252]{2,1,0:T(8,128)(2,1)} %pad_maximum_fusion), calls=%async_computation.3 | async-start | bytes 2162688 | tf_op jit(solution)/shard_map/all_to_all | solution.py:36
  117.4 0.2 reduce_sum.21
  117.6 10.5 %all_gather.6 = bf16[32,2016]{1,0:T(8,128)(2,1)S(1)} all-gather(bf16[8,2016]{1,0:T(8,128)(2,1)S(1)} %reduce_sum.21), channel_id=1, replica_groups=mesh['fs'=24,'tp_0'=8,'tp_1'=4] {'tp_1'}, dimensions={0}, use_global_device_ids=true | all-gather | bytes 161280 | tf_op jit(solution)/shard_map/all_gather | solution.py:42
  128.0 22.4 %all_gather.7 = bf16[256,2016]{1,0:T(8,128)(2,1)S(1)} all-gather(bf16[32,2016]{1,0:T(8,128)(2,1)S(1)} %all_gather.6), channel_id=1, replica_groups=mesh['fs'=24,'tp_0'=8,'tp_1'=4] {'tp_0'}, dimensions={0}, use_global_device_ids=true | all-gather | bytes 1161216 | tf_op jit(solution)/shard_map/all_gather | solution.py:42
  150.4 1.3 copy.11
  151.8 5.2 %all-to-all-done.3 = bf16[24,84,252]{2,1,0:T(8,128)(2,1)S(1)} async-done(((bf16[24,84,252]{2,1,0:T(8,128)(2,1)}), bf16[24,84,252]{2,1,0:T(8,128)(2,1)S(1)}, u32[]{:S(2)}, u32[]{:S(2)}) %all-to-all-start.3) | async-done | bytes 1016096 | tf_op jit(solution)/shard_map/all_to_all | solution.py:36
  157.0 0.2 convert_reduce_fusion
  157.2 0.7 slice_bitcast_fusion
  (7 shorter events, 0.1 us)
Async XLA Ops:
  0.6 47.7 %copy-start = (bf16[256,2016]{0,1:T(8,128)(2,1)S(1)}, bf16[256,2016]{0,1:T(8,128)(2,1)}, u32[]{:S(2)}) copy-start(bf16[256,2016]{0,1:T(8,128)(2,1)} %param.7) | copy-start | bytes 3096580
  0.6 40.5 %copy-start.2 = (bf16[84,126]{1,0:T(8,128)(2,1)S(1)}, bf16[84,126]{1,0:T(8,128)(2,1)}, u32[]{:S(2)}) copy-start(bf16[84,126]{1,0:T(8,128)(2,1)} %param.8) | copy-start | bytes 63508
  42.0 6.3 %copy-start.1 = (bf16[256,126]{1,0:T(8,128)(2,1)S(1)}, bf16[256,126]{1,0:T(8,128)(2,1)}, u32[]{:S(2)}) copy-start(bf16[256,126]{1,0:T(8,128)(2,1)} %param.6) | copy-start | bytes 193540
  42.0 29.2 %all-to-all-start.1 = ((bf16[24,84,126]{2,1,0:T(8,128)(2,1)}), bf16[24,84,126]{2,1,0:T(8,128)(2,1)S(1)}, u32[]{:S(2)}, u32[]{:S(2)}) async-start(bf16[24,84,126]{2,1,0:T(8,128)(2,1)} %broadcast_in_dim.5), calls=%async_computation.1 | async-start | bytes 1081344 | tf_op jit(solution)/shard_map/all_to_all | solution.py:12
  73.3 34.6 %all-to-all-start.2 = ((bf16[32,8,2016]{2,1,0:T(8,128)(2,1)}), bf16[32,8,2016]{2,1,0:T(8,128)(2,1)S(1)}, u32[]{:S(2)}, u32[]{:S(2)}) async-start(bf16[32,8,2016]{2,1,0:T(8,128)(2,1)} %bitcast.1), calls=%async_computation.2 | async-start | bytes 2097152 | tf_op jit(solution)/shard_map/all_to_all | solution.py:36
  107.8 49.1 %all-to-all-start.3 = ((bf16[24,84,252]{2,1,0:T(8,128)(2,1)}), bf16[24,84,252]{2,1,0:T(8,128)(2,1)S(1)}, u32[]{:S(2)}, u32[]{:S(2)}) async-start(bf16[24,84,252]{2,1,0:T(8,128)(2,1)} %pad_maximum_fusion), calls=%async_computation.3 | async-start | bytes 2162688 | tf_op jit(solution)/shard_map/all_to_all | solution.py:36
where the time goes:
time: 160 us; the launch traced here: 158 us
  blocking collectives  72.4 us (45%)
  waiting for transfers between devices  46.9 us (29%)
  starting transfers between devices  25.3 us (16%)
  local copies, waits for them, and re-layouts  6.9 us (4%)
  matrix products  3.78 us (2%)
  other arithmetic  1.82 us (1%)
    all_to_all x1, blocking collectives, sent_to_all(): lax.all_to_all(jnp.broadcast_to(value[None], (length, *value.shape)), axi...  39.6 us
    all_gather x2, blocking collectives, gathered_by_axis(): value = lax.all_gather(value, axis, axis=dim, tiled=True)  32.9 us
    all_to_all x2, waiting for transfers between devices, sent_and_summed(): lax.all_to_all(split_up(value, dim, length), axis, 0, 0, tiled=True)  24.5 us
    all_to_all x1, waiting for transfers between devices, sent_to_all(): lax.all_to_all(jnp.broadcast_to(value[None], (length, *value.shape)), axi...  22.4 us
    all_to_all x2, starting transfers between devices, sent_and_summed(): lax.all_to_all(split_up(value, dim, length), axis, 0, 0, tiled=True)  19.2 us
    all_to_all x1, starting transfers between devices, sent_to_all(): lax.all_to_all(jnp.broadcast_to(value[None], (length, *value.shape)), axi...  6.12 us
  transfers between devices with their start and end apart: 3, of which 3 were waited for; matrix products, arithmetic and copies ran while one was open for 5% of the time, Pallas kernels for 0%

commit v1 on v0

v1 whole, which is shorter than its diff:
```python
import functools

import jax
import jax.numpy as jnp
from jax import lax
from jax.experimental import pallas as pl
from jax.experimental.pallas import tpu as pltpu
from jax.sharding import Mesh
from jax.sharding import PartitionSpec as P

AXES = ("z", "c", "y", "x")
NZ, NC, NY, NX = 12, 2, 8, 4
MESH_IDS = pl.DeviceIdType.MESH
F32 = jnp.float32
BF16 = jnp.bfloat16
TOK, D, WID, BLK = 256, 2016, 126, 84
DP, ROWS = 2048, 96
CHUNKS = 4
CR = TOK // NX // CHUNKS
YL = DP // NY


def kernel(
    inputs_hbm, pre_hbm, cot_hbm, wup_hbm, wdown_hbm,
    gi_out, gup_out, gdown_out,
    inp, pre, cot, wup, wdn,
    scr, pact, wc, grad, wg, pgrad, part, xr, xs, yr, gi,
    gs, sib, cs, zr,
    ld_sem, out_sem, ag_recv, ag_sib, ag_send,
    sib_send, sib_recv, z_send, z_recv,
    x_send, x_recv, y_send, y_recv, ay_send, ay_recv, ax_send, ax_recv,
):
    z, c, y, x = (lax.axis_index(a) for a in AXES)

    def zpeer(d):
        return {"z": lax.rem(z + (d + NZ), NZ)}

    def ypeer(d):
        return {"y": lax.rem(y + d, NY)}

    def xpeer(d):
        return {"x": lax.rem(x + d, NX)}

    other = {"c": 1 - c}

    def send(src, dst, ssem, rsem, to):
        pltpu.make_async_remote_copy(
            src_ref=src, dst_ref=dst, send_sem=ssem, recv_sem=rsem,
            device_id=to, device_id_type=MESH_IDS,
        ).start()

    def wait(ref, sem):
        pltpu.make_async_copy(ref, ref, sem).wait()

    loads = [
        pltpu.make_async_copy(a, b, ld_sem.at[i])
        for i, (a, b) in enumerate(
            ((wdown_hbm, wdn), (wup_hbm, wup), (pre_hbm, pre), (cot_hbm, cot), (inputs_hbm, inp))
        )
    ]
    for copy in loads:
        copy.start()

    barrier = pltpu.get_barrier_semaphore()
    peers = [zpeer(d) for d in range(1, NZ)] + [other]
    peers += [xpeer(d) for d in range(1, NX)] + [ypeer(d) for d in range(1, NY)]
    for to in peers:
        pl.semaphore_signal(barrier, inc=1, device_id=to, device_id_type=MESH_IDS)

    mine = 2 * z + c
    scr[...] = jnp.zeros_like(scr)
    loads[0].wait()
    scr[0:WID, 0:BLK] = wdn[...].astype(F32)
    wg[0, mine] = scr[...].T[0:ROWS].astype(BF16)
    scr[...] = jnp.zeros_like(scr)
    loads[1].wait()
    scr[0:BLK, 0:WID] = wup[...].astype(F32)
    wg[1, mine] = scr[0:ROWS].astype(BF16)

    pl.semaphore_wait(barrier, len(peers))

    def block_from(d):
        return 2 * lax.rem(z - d + NZ, NZ) + c

    def ag_first(w):
        ref = wg.at[w, mine]
        for d in (3, -3, 2, -2, 1, -1):
            send(ref, ref, ag_send.at[w], ag_recv.at[w, d % NZ], zpeer(d))
        send(ref, ref, ag_send.at[w], ag_sib.at[w, 0], other)

    def ag_arrived(w, d):
        ref = wg.at[w, block_from(d)]
        wait(ref, ag_recv.at[w, d % NZ])

    def ag_pass(w, d):
        ref = wg.at[w, block_from(d)]
        send(ref, ref, ag_send.at[w], ag_sib.at[w, d % NZ], other)

    def ag_relay(w):
        for d in (3, -3):
            ag_arrived(w, d)
        far = wg.at[w, 2 * lax.rem(z + (NZ - 3) + 6 * c, NZ) + c]
        send(far, far, ag_send.at[w], ag_recv.at[w, 6], {"z": lax.rem(z + (NZ + 3) - 6 * c, NZ)})
        for step in (2, 1):
            for s in (1, -1):
                ref = wg.at[w, block_from(3 * s)]
                d = s * (3 + step)
                send(ref, ref, ag_send.at[w], ag_recv.at[w, d % NZ], zpeer(s * step))
        for d in (3, -3):
            ag_pass(w, d)

    def ag_near(w):
        for d in (2, -2, 1, -1):
            ag_arrived(w, d)
            ag_pass(w, d)

    def ag_far(w):
        for d in (4, -4, 5, -5, 6):
            ag_arrived(w, d)
            ag_pass(w, d)

    def ag_last(w):
        for d in range(NZ):
            ref = wg.at[w, 2 * lax.rem(z - d + NZ, NZ) + 1 - c]
            wait(ref, ag_sib.at[w, d])

    def compact(w):
        for f in range(2 * NZ):
            wc[f * BLK : f * BLK + ROWS, :] = wg[w, f].astype(F32)

    def to_blocks(g):
        for f in range(2 * NZ):
            gs[g, f % 2, f // 2] = grad[f * BLK : f * BLK + ROWS, :].astype(BF16)

    def pair_send(g):
        send(gs.at[g, 1 - c], sib.at[g], sib_send.at[g], sib_recv.at[g], other)

    def pair_sum(g):
        wait(sib.at[g], sib_recv.at[g])
        for k in range(NZ):
            cs[g, k] = (gs[g, c, k].astype(F32) + sib[g, k].astype(F32)).astype(BF16)

    def z_out(g):
        for d in (6, 5, -5, 4, -4, 3, -3, 2, -2, 1, -1):
            to = lax.rem(z + (d + NZ), NZ)
            send(cs.at[g, to], zr.at[g, d % NZ - 1], z_send.at[g], z_recv.at[g], {"z": to})

    def z_sum(g):
        wait(zr.at[g], z_recv.at[g])
        total = cs[g, z].astype(F32)
        for k in range(NZ - 1):
            total = total + zr[g, k].astype(F32)
        return total

    ag_first(0)
    ag_first(1)

    wc[2016:DP, :] = jnp.zeros((DP - 2016, 128), F32)
    grad[2016:DP, :] = jnp.zeros((DP - 2016, 128), F32)
    pact[...] = jnp.zeros_like(pact)
    loads[2].wait()
    pact[:, 0:WID] = jnp.maximum(pre[...].astype(F32), 0.0)
    positive = pact[...]
    hidden = (positive * positive).astype(BF16)
    ag_relay(0)
    loads[3].wait()
    grad[0:D, :] = lax.dot_general(
        cot[...], hidden, (((0,), (0,)), ((), ())), preferred_element_type=F32
    )
    to_blocks(0)
    pair_send(0)
    ag_near(0)
    ag_relay(1)
    ag_near(1)
    ag_far(0)
    ag_last(0)
    compact(0)
    hidden_grad = jnp.dot(cot[...], wc[0:D, :].astype(BF16), preferred_element_type=F32)
    pgrad[...] = (2.0 * pact[...] * hidden_grad).astype(BF16)
    ag_far(1)
    ag_last(1)
    compact(1)

    def rows_of(share, k):
        return pl.ds(pl.multiple_of(share * (TOK // NX) + k * CR, CR), CR)

    weights = wc[...].astype(BF16)
    part[...] = lax.dot_general(
        pgrad[...], weights, (((1,), (1,)), ((), ())), preferred_element_type=F32
    ).astype(BF16)
    for k in range(CHUNKS):
        for d in (2, 1, 3):
            to = lax.rem(x + d, NX)
            send(part.at[rows_of(to, k), :], xr.at[k, d - 1], x_send.at[k], x_recv.at[k], {"x": to})

    pair_sum(0)
    z_out(0)
    loads[4].wait()
    grad[0:D, :] = lax.dot_general(
        inp[...], pgrad[...], (((0,), (0,)), ((), ())), preferred_element_type=F32
    )
    to_blocks(1)
    pair_send(1)

    def own_lanes(who):
        return pl.ds(pl.multiple_of(who * YL, YL), YL)

    def x_step(k):
        wait(xr.at[k], x_recv.at[k])
        total = part[rows_of(x, k), :].astype(F32)
        for j in range(NX - 1):
            total = total + xr[k, j].astype(F32)
        xs[k] = total.astype(BF16)
        for d in (4, 3, 5, 2, 6, 1, 7):
            to = lax.rem(y + d, NY)
            send(xs.at[k, :, own_lanes(to)], yr.at[k, d - 1], y_send.at[k], y_recv.at[k], {"y": to})

    def y_step(k):
        wait(yr.at[k], y_recv.at[k])
        total = xs[k, :, own_lanes(y)].astype(F32)
        for j in range(NY - 1):
            total = total + yr[k, j].astype(F32)
        gi[rows_of(x, k), own_lanes(y)] = total.astype(BF16)
        ref = gi.at[rows_of(x, k), own_lanes(y)]
        for d in (4, 3, 5, 2, 6, 1, 7):
            send(ref, ref, ay_send.at[k], ay_recv.at[k], ypeer(d))

    def ay_step(k):
        wait(yr.at[k], ay_recv.at[k])
        ref = gi.at[rows_of(x, k), :]
        for d in (2, 1, 3):
            send(ref, ref, ax_send.at[k], ax_recv.at[k], xpeer(d))

    def ax_step(k):
        wait(xr.at[k], ax_recv.at[k])
        for s in range(NX):
            rows = slice(s * (TOK // NX) + k * CR, s * (TOK // NX) + (k + 1) * CR)
            pltpu.make_async_copy(gi.at[rows, :], gi_out.at[rows, :], out_sem.at[k, s]).start()

    x_step(0)
    x_step(1)
    pair_sum(1)
    z_out(1)
    y_step(0)
    x_step(2)
    y_step(1)
    x_step(3)
    ay_step(0)
    y_step(2)
    ay_step(1)
    y_step(3)
    ay_step(2)
    ax_step(0)
    ay_step(3)
    ax_step(1)
    down = z_sum(0)
    scr[...] = jnp.zeros_like(scr)
    scr[0:ROWS, :] = down
    gdown_out[...] = scr[...].T[0:WID, 0:BLK]
    ax_step(2)
    gup_out[...] = z_sum(1)[0:BLK, 0:WID]
    ax_step(3)

    for w in range(2):
        wait(wg.at[w, pl.ds(0, 23)], ag_send.at[w])
        wait(sib.at[w], sib_send.at[w])
        wait(zr.at[w], z_send.at[w])
    for k in range(CHUNKS):
        wait(xr.at[k], x_send.at[k])
        wait(yr.at[k], y_send.at[k])
        wait(yr.at[k], ay_send.at[k])
        wait(xr.at[k], ax_send.at[k])
        for s in range(NX):
            rows = slice(s * (TOK // NX) + k * CR, s * (TOK // NX) + (k + 1) * CR)
            pltpu.make_async_copy(gi.at[rows, :], gi_out.at[rows, :], out_sem.at[k, s]).wait()


def on_device(inputs, pre_act, cotangent, w_up, w_down):
    any_space = pl.BlockSpec(memory_space=pl.ANY)
    in_vmem = pl.BlockSpec(memory_space=pltpu.VMEM)
    dma = pltpu.SemaphoreType.DMA
    grad_input, grad_up, grad_down = pl.pallas_call(
        kernel,
        out_shape=(
            jax.ShapeDtypeStruct((TOK, DP), BF16),
            jax.ShapeDtypeStruct((BLK, WID), F32),
            jax.ShapeDtypeStruct((WID, BLK), F32),
        ),
        in_specs=[any_space] * 5,
        out_specs=(any_space, in_vmem, in_vmem),
        scratch_shapes=[
            pltpu.VMEM((TOK, D), BF16),
            pltpu.VMEM((TOK, WID), BF16),
            pltpu.VMEM((TOK, D), BF16),
            pltpu.VMEM((BLK, WID), BF16),
            pltpu.VMEM((WID, BLK), BF16),
            pltpu.VMEM((128, 128), F32),
            pltpu.VMEM((TOK, 128), F32),
            pltpu.VMEM((DP, 128), F32),
            pltpu.VMEM((DP, 128), F32),
            pltpu.VMEM((2, 2 * NZ, ROWS, 128), BF16),
            pltpu.VMEM((TOK, 128), BF16),
            pltpu.VMEM((TOK, DP), BF16),
            pltpu.VMEM((CHUNKS, NX - 1, CR, DP), BF16),
            pltpu.VMEM((CHUNKS, CR, DP), BF16),
            pltpu.VMEM((CHUNKS, NY - 1, CR, YL), BF16),
            pltpu.VMEM((TOK, DP), BF16),
            pltpu.VMEM((2, 2, NZ, ROWS, 128), BF16),
            pltpu.VMEM((2, NZ, ROWS, 128), BF16),
            pltpu.VMEM((2, NZ, ROWS, 128), BF16),
            pltpu.VMEM((2, NZ - 1, ROWS, 128), BF16),
            dma((5,)), dma((CHUNKS, NX)), dma((2, NZ)), dma((2, NZ)), dma((2,)),
            dma((2,)), dma((2,)), dma((2,)), dma((2,)),
            dma((CHUNKS,)), dma((CHUNKS,)), dma((CHUNKS,)), dma((CHUNKS,)),
            dma((CHUNKS,)), dma((CHUNKS,)), dma((CHUNKS,)), dma((CHUNKS,)),
        ],
        compiler_params=pltpu.CompilerParams(
            collective_id=0, has_side_effects=True, vmem_limit_bytes=48 << 20
        ),
    )(inputs, pre_act, cotangent, w_up, w_down)
    return grad_input[:, :D], grad_up, grad_down


def solution(mesh):
    split = Mesh(mesh.devices.reshape(NZ, NC, NY, NX), AXES)
    fs, tp = ("z", "c"), ("y", "x")
    return jax.shard_map(
        on_device,
        mesh=split,
        in_specs=(P(fs, None), P(fs, tp), P(fs, None), P(fs, tp), P(tp, fs)),
        out_specs=(P(fs, None), P(fs, tp), P(tp, fs)),
        check_vma=False,
    )
```

time: 160 us -> 70.2 us (0.44)
  blocking collectives: 72.4 us -> 0 us
  Pallas kernels: 0 us -> 62.2 us
  waiting for transfers between devices: 46.9 us -> 0 us
  starting transfers between devices: 25.3 us -> 0 us
  matrix products: 3.78 us -> 0 us
  other arithmetic: 1.82 us -> 0 us
    pallas_call x0 -> x1, Pallas kernels: none -> 62.2 us  [on_device(): pl.pallas_call(kernel, out_shape=(jax.ShapeDtypeStruct((TOK, DP), BF16),...]
    all_to_all x3 -> x0, waiting for transfers between devices: 46.9 us -> none  [the longest x2 24.5 us: sent_and_summed(): lax.all_to_all(split_up(value, dim, length), axis, 0, 0, tiled=True)]
    all_to_all x1 -> x0, blocking collectives: 39.6 us -> none  [sent_to_all(): lax.all_to_all(jnp.broadcast_to(value[None], (length, *value.shape)), axi...]
    all_gather x2 -> x0, blocking collectives: 32.9 us -> none  [gathered_by_axis(): value = lax.all_gather(value, axis, axis=dim, tiled=True)]
    all_to_all x3 -> x0, starting transfers between devices: 25.3 us -> none  [the longest x2 19.2 us: sent_and_summed(): lax.all_to_all(split_up(value, dim, length), axis, 0, 0, tiled=True)]
    unnamed x7 -> x12, local copies, waits for them, and re-layouts: 1.35 us -> 5.93 us
    dot_general x4 -> x0, matrix products: 3.78 us -> none  [the longest x1 2.44 us: on_device(): lax.dot_general(columns, pre_grad, (((0,), (0,)), ((), ())), preferred_el...]
    broadcast_in_dim x2 -> x0, local copies, waits for them, and re-layouts: 1.76 us -> none  [sent_to_all(): jnp.broadcast_to(value[None], (length, *value.shape))]
  transfers between devices with their start and end apart: 3 -> 0, of which waited for: 3 -> 0; matrix products, arithmetic and copies ran while one was open for 5% -> 0% of each run, Pallas kernels for 0% -> 0%
where the time goes in v1:
time: 70.2 us; the launch traced here: 68.8 us
  Pallas kernels  62.2 us (89%)
  local copies, waits for them, and re-layouts  5.93 us (8%)
    pallas_call x1, Pallas kernels, on_device(): pl.pallas_call(kernel, out_shape=(jax.ShapeDtypeStruct((TOK, DP), BF16),...  62.2 us
    unnamed x12, local copies, waits for them, and re-layouts  5.93 us

profile of v1, /device:TPU:1, one launch (start us, length us, event | category | flops | bytes accessed | tf_op | source)
XLA Modules:
  0.0 68.8 jit_solution(9553151464957484575)
XLA Ops:
  0.6 0.9 %copy.10.wdown_hbm = bf16[126,84]{1,0:T(8,128)(2,1)S(1)} copy(bf16[126,84]{0,1:T(8,128)(2,1)} %param.9) | data formatting | bytes 42336 | tf_op args[4]
  1.5 0.0 copy-start.2
  1.5 1.6 %copy.8.inputs_hbm = bf16[256,2016]{1,0:T(8,128)(2,1)S(1)} copy(bf16[256,2016]{0,1:T(8,128)(2,1)} %param.5) | data formatting | bytes 2064384 | tf_op args[0]
  3.1 0.0 copy-done.2
  3.1 0.0 copy-start
  3.1 0.0 copy-start.1
  3.1 0.6 copy.9.cot_hbm
  3.8 0.2 copy-done
  3.9 0.0 copy-done.1
  3.9 62.2 %shard_map.76 = (bf16[256,2048]{1,0:T(8,128)(2,1)S(1)}, f32[84,126]{1,0:T(8,128)S(1)}, f32[126,84]{1,0:T(8,128)S(1)}) custom-call(bf16[256,2016]{1,0:T(8,128)(2,1)S(1)} %copy.8.inputs_hbm, bf16[256,126]{1,0:T(8,128)(2,1)S(1)} %copy-done, bf16[256,2016]{1,0:T(8,128)(2,1)S(1)} %copy.9.cot_hbm, bf16[84,126]{1,0:T(8,128)(2,1)S(1)} %copy-done.1, ...), custom_call_target="tpu_custom_call" | custom-call | tf_op jit(solution)/shard_map/pallas_call | solution.py:282
  66.1 1.3 %copy.11 = bf16[256,2016]{0,1:T(8,128)(2,1)} copy(bf16[256,2016]{1,0:T(8,128)(2,1)S(1)} %bitcast.1) | data formatting | bytes 2064384
  67.5 0.7 %copy.12 = f32[126,84]{0,1:T(8,128)} copy(f32[126,84]{1,0:T(8,128)S(1)} %get-tuple-element.11) | data formatting | bytes 84672
  68.2 0.6 copy.14
Async XLA Ops:
  1.5 1.6 %copy-start.2 = (bf16[256,2016]{0,1:T(8,128)(2,1)S(1)}, bf16[256,2016]{0,1:T(8,128)(2,1)}, u32[]{:S(2)}) copy-start(bf16[256,2016]{0,1:T(8,128)(2,1)} %param.7) | copy-start | bytes 3096580
  3.1 0.8 %copy-start = (bf16[256,126]{1,0:T(8,128)(2,1)S(1)}, bf16[256,126]{1,0:T(8,128)(2,1)}, u32[]{:S(2)}) copy-start(bf16[256,126]{1,0:T(8,128)(2,1)} %pre_hbm.1) | copy-start | bytes 193540
  3.1 0.8 %copy-start.1 = (bf16[84,126]{1,0:T(8,128)(2,1)S(1)}, bf16[84,126]{1,0:T(8,128)(2,1)}, u32[]{:S(2)}) copy-start(bf16[84,126]{1,0:T(8,128)(2,1)} %wup_hbm.1) | copy-start | bytes 63508

commit v2 on v1

v2 whole, which is shorter than its diff:
```python
import functools

import jax
import jax.numpy as jnp
from jax import lax
from jax.experimental import pallas as pl
from jax.experimental.pallas import tpu as pltpu
from jax.sharding import Mesh
from jax.sharding import PartitionSpec as P

AXES = ("z", "c", "y", "x")
NZ, NC, NY, NX = 12, 2, 8, 4
MESH_IDS = pl.DeviceIdType.MESH
F32 = jnp.float32
BF16 = jnp.bfloat16
TOK, D, WID, BLK = 256, 2016, 126, 84
DP, ROWS = 2048, 96
LANES, QUARTERS, RB = 128, 4, 16
CHUNKS = [(h, q) for h in range(TOK // LANES) for q in range(QUARTERS)]
Y_FIRST = (1,)
X_FIRST = tuple(i for i in range(len(CHUNKS)) if i not in Y_FIRST)
ORDER = tuple(range(len(CHUNKS)))
X_TIMES = (3.8, 8.4, 13.0)
Y_TIMES = (7.5, 11.0, 14.5)
X_STEP, Y_STEP = 1.4, 3.0


def kernel(
    inputs_hbm, pre_hbm, cot_hbm, wup_hbm, wdown_hbm,
    gi, gup_out, gdown_out,
    inp, pre, cot, wup, wdn,
    cotn, scr, pact, wc, grad, wg, pgrad, pgt, part,
    x_in1, x_sum, y_in2, y_in1, y_sum, x_in2,
    gs, sib, cs, zr,
    ld_sem, ag_recv, ag_sib, ag_send,
    sib_send, sib_recv, z_send, z_recv,
    s1, r1, s2, r2, s3, r3, s4, r4,
):
    z, c, y, x = (lax.axis_index(a) for a in AXES)

    def zpeer(d):
        return {"z": lax.rem(z + (d + NZ), NZ)}

    def ypeer(d):
        return {"y": lax.rem(y + d, NY)}

    def xpeer(d):
        return {"x": lax.rem(x + d, NX)}

    other = {"c": 1 - c}

    def send(src, dst, ssem, rsem, to):
        pltpu.make_async_remote_copy(
            src_ref=src, dst_ref=dst, send_sem=ssem, recv_sem=rsem,
            device_id=to, device_id_type=MESH_IDS,
        ).start()

    def wait(ref, sem):
        pltpu.make_async_copy(ref, ref, sem).wait()

    loads = [
        pltpu.make_async_copy(a, b, ld_sem.at[i])
        for i, (a, b) in enumerate(
            ((wdown_hbm, wdn), (wup_hbm, wup), (pre_hbm, pre), (cot_hbm, cot), (inputs_hbm, inp))
        )
    ]
    for copy in loads:
        copy.start()

    barrier = pltpu.get_barrier_semaphore()
    peers = [zpeer(d) for d in (2, -2, 1, -1)] + [other]
    peers += [xpeer(d) for d in range(1, NX)] + [ypeer(d) for d in range(1, NY)]
    for to in peers:
        pl.semaphore_signal(barrier, inc=1, device_id=to, device_id_type=MESH_IDS)

    mine = 2 * z + c
    scr[...] = jnp.zeros_like(scr)
    loads[0].wait()
    scr[0:BLK, 0:WID] = wdn[...].astype(F32)
    wg[0, mine] = scr[...].astype(BF16)
    loads[1].wait()
    scr[0:BLK, 0:WID] = wup[...].astype(F32)
    wg[1, mine] = scr[...].astype(BF16)

    pl.semaphore_wait(barrier, len(peers))

    def block_from(d):
        return 2 * lax.rem(z - d + NZ, NZ) + c

    def ag_own(w, *steps):
        ref = wg.at[w, mine]
        for d in steps:
            send(ref, ref, ag_send.at[w], ag_recv.at[w, d % NZ], zpeer(d))

    def ag_own_pair(w):
        ref = wg.at[w, mine]
        send(ref, ref, ag_send.at[w], ag_sib.at[w, 0], other)

    def ag_wait(w, *ds):
        for d in ds:
            wait(wg.at[w, block_from(d)], ag_recv.at[w, d % NZ])

    def ag_relay(w, d, *steps):
        ref = wg.at[w, block_from(d)]
        for step in steps:
            send(ref, ref, ag_send.at[w], ag_recv.at[w, (d + step) % NZ], zpeer(step))

    def ag_far(w, d):
        @pl.when(c == (0 if d > 0 else 1))
        def _():
            ref = wg.at[w, block_from(d)]
            step = 2 if d > 0 else -2
            send(ref, ref, ag_send.at[w], ag_recv.at[w, 6], zpeer(step))

    def ag_pass(w, *ds):
        for d in ds:
            ref = wg.at[w, block_from(d)]
            send(ref, ref, ag_send.at[w], ag_sib.at[w, d % NZ], other)

    def ag_last(w):
        for d in range(NZ):
            ref = wg.at[w, 2 * lax.rem(z - d + NZ, NZ) + 1 - c]
            wait(ref, ag_sib.at[w, d])

    def compact(w):
        for f in range(2 * NZ):
            wc[f * BLK : f * BLK + ROWS, :] = wg[w, f].astype(F32)

    def to_blocks(g):
        for f in range(2 * NZ):
            gs[g, f % 2, f // 2] = grad[f * BLK : f * BLK + ROWS, :].astype(BF16)

    def pair_send(g):
        send(gs.at[g, 1 - c], sib.at[g], sib_send.at[g], sib_recv.at[g], other)

    def pair_sum(g):
        wait(sib.at[g], sib_recv.at[g])
        for k in range(NZ):
            cs[g, k] = (gs[g, c, k].astype(F32) + sib[g, k].astype(F32)).astype(BF16)

    def z_out(g):
        for d in (6, 5, -5, 4, -4, 3, -3, 2, -2, 1, -1):
            to = lax.rem(z + (d + NZ), NZ)
            send(cs.at[g, to], zr.at[g, d % NZ - 1], z_send.at[g], z_recv.at[g], {"z": to})

    def z_sum(g):
        wait(zr.at[g], z_recv.at[g])
        total = cs[g, z].astype(F32)
        for k in range(NZ - 1):
            total = total + zr[g, k].astype(F32)
        return total

    for w in range(2):
        ag_own(w, 2, -2)
    for w in range(2):
        ag_own_pair(w)

    wc[D:DP, :] = jnp.zeros((DP - D, 128), F32)
    grad[D:DP, :] = jnp.zeros((DP - D, 128), F32)
    pact[...] = jnp.zeros_like(pact)
    loads[2].wait()
    pact[:, 0:WID] = jnp.maximum(pre[...].astype(F32), 0.0)
    positive = pact[...]
    hidden = (positive * positive).astype(BF16)
    loads[3].wait()
    cotn[...] = cot[...].T
    grad[0:D, :] = jnp.dot(cot[...], hidden, preferred_element_type=F32)
    to_blocks(0)
    pair_send(0)

    for w in range(2):
        for d in (2, -2):
            ag_wait(w, d)
            ag_relay(w, d, d)
    for w in range(2):
        ag_own(w, 1, -1)
        ag_pass(w, 2, -2)
    pair_sum(0)
    for w in range(2):
        for d in (4, -4):
            ag_wait(w, d)
            ag_far(w, d)
            ag_relay(w, d, d // 4)
    for w in range(2):
        for d in (2, -2):
            ag_relay(w, d, d // 2)
        ag_pass(w, 4, -4)
    for w in range(2):
        for d in (1, -1):
            ag_wait(w, d)
            ag_pass(w, d)
    for w in range(2):
        for d in (6, 5, -5, 3, -3):
            ag_wait(w, d)
            ag_pass(w, d)
    z_out(0)
    ag_last(0)
    compact(0)
    hidden_grad = jnp.dot(cotn[...], wc[0:D, :].astype(BF16), preferred_element_type=F32)
    pre_grad = 2.0 * pact[...] * hidden_grad
    pgrad[...] = pre_grad.astype(BF16)
    pgt[...] = pre_grad.T.astype(BF16)
    ag_last(1)
    compact(1)

    def others(n):
        return sorted(range(1, n), key=lambda d: -min(d, n - d))

    def scatter(n, me, axis, src, dst, ssem, rsem):
        for d in others(n):
            to = lax.rem(me + d, n)
            send(src(to), dst.at[d - 1], ssem, rsem, {axis: to})

    def share(n, me, axis, ref, ssem, rsem):
        for d in others(n):
            send(ref, ref, ssem, rsem, {axis: lax.rem(me + d, n)})

    def total(own, arrived):
        out = own.astype(F32)
        for j in range(arrived.shape[0]):
            out = out + arrived[j].astype(F32)
        return out.astype(BF16)

    def stage0(i):
        h, q = CHUNKS[i]
        for s in range(NX):
            start = (s * QUARTERS + q) * NY * RB
            rows = wc[start : start + NY * RB, :].astype(BF16)
            half = pgt[:, h * LANES : (h + 1) * LANES]
            product = jnp.dot(rows, half, preferred_element_type=F32).astype(BF16)
            part[h, s, q] = product.reshape(NY, RB, LANES)
        if i in Y_FIRST:
            dst = y_in1.at[Y_FIRST.index(i)]
            scatter(NY, y, "y", lambda to: part.at[h, :, q, to], dst, s1.at[i], r1.at[i])
        else:
            dst = x_in1.at[X_FIRST.index(i)]
            scatter(NX, x, "x", lambda to: part.at[h, to, q], dst, s1.at[i], r1.at[i])

    def stage1(i):
        h, q = CHUNKS[i]
        if i in Y_FIRST:
            j = Y_FIRST.index(i)
            wait(y_in1.at[j], r1.at[i])
            y_sum[j] = total(part[h, :, q, y], y_in1.at[j])
            scatter(NX, x, "x", lambda to: y_sum.at[j, to], x_in2.at[j], s2.at[i], r2.at[i])
        else:
            j = X_FIRST.index(i)
            wait(x_in1.at[j], r1.at[i])
            x_sum[j] = total(part[h, x, q], x_in1.at[j])
            scatter(NY, y, "y", lambda to: x_sum.at[j, to], y_in2.at[j], s2.at[i], r2.at[i])

    def stage2(i):
        h, q = CHUNKS[i]
        ref = gi.at[h, x, q, y]
        if i in Y_FIRST:
            j = Y_FIRST.index(i)
            wait(x_in2.at[j], r2.at[i])
            gi[h, x, q, y] = total(y_sum[j, x], x_in2.at[j])
            share(NX, x, "x", ref, s3.at[i], r3.at[i])
        else:
            j = X_FIRST.index(i)
            wait(y_in2.at[j], r2.at[i])
            gi[h, x, q, y] = total(x_sum[j, y], y_in2.at[j])
            share(NY, y, "y", ref, s3.at[i], r3.at[i])

    def stage3(i):
        h, q = CHUNKS[i]
        if i in Y_FIRST:
            wait(x_in2.at[Y_FIRST.index(i)], r3.at[i])
            share(NY, y, "y", gi.at[h, :, q, y], s4.at[i], r4.at[i])
        else:
            wait(y_in2.at[X_FIRST.index(i)], r3.at[i])
            share(NX, x, "x", gi.at[h, x, q], s4.at[i], r4.at[i])

    def finish(i):
        if i in Y_FIRST:
            j = Y_FIRST.index(i)
            first, second = y_in1.at[j], x_in2.at[j]
        else:
            j = X_FIRST.index(i)
            first, second = x_in1.at[j], y_in2.at[j]
        wait(first, r4.at[i])
        wait(first, s1.at[i])
        wait(second, s2.at[i])
        wait(second, s3.at[i])
        wait(first, s4.at[i])

    for i in ORDER:
        stage0(i)

    loads[4].wait()
    grad[0:D, :] = jnp.dot(inp[...], pgrad[...], preferred_element_type=F32)
    to_blocks(1)
    pair_send(1)

    events = []
    for group, times, step in ((X_FIRST, X_TIMES, X_STEP), (Y_FIRST, Y_TIMES, Y_STEP)):
        for n, stage in enumerate((stage1, stage2, stage3)):
            events += [(times[n] + step * j, i, stage) for j, i in enumerate(group)]
    events.sort(key=lambda e: e[:2])
    for t, (_, i, stage) in enumerate(events):
        stage(i)
        if t == 0:
            pair_sum(1)
            z_out(1)
    gdown_out[...] = z_sum(0)[0:BLK, 0:WID]
    gup_out[...] = z_sum(1)[0:BLK, 0:WID]
    for w in range(2):
        wait(wg.at[w, pl.ds(0, 23)], ag_send.at[w])
        wait(sib.at[w], sib_send.at[w])
        wait(zr.at[w], z_send.at[w])
    for i in ORDER:
        finish(i)


def store(gi, gup, gdown, gi_out, gup_out, gdown_out, sem):
    pairs = [
        (gi.at[h, pl.ds(0, D)], gi_out.at[:, pl.ds(h * LANES, LANES)])
        for h in range(TOK // LANES)
    ]
    pairs += [(gup, gup_out), (gdown, gdown_out)]
    copies = [pltpu.make_async_copy(a, b, sem.at[i]) for i, (a, b) in enumerate(pairs)]
    for copy in copies:
        copy.start()
    for copy in copies:
        copy.wait()


def on_device(inputs, pre_act, cotangent, w_up, w_down):
    in_hbm = pl.BlockSpec(memory_space=pltpu.HBM)
    in_vmem = pl.BlockSpec(memory_space=pltpu.VMEM)
    dma = pltpu.SemaphoreType.DMA
    operands = [
        pltpu.with_memory_space_constraint(a, pltpu.HBM)
        for a in (inputs.T, pre_act, cotangent.T, w_up, w_down.T)
    ]
    grad_input, grad_up, grad_down = pl.pallas_call(
        kernel,
        out_shape=(
            jax.ShapeDtypeStruct((TOK // LANES, NX, QUARTERS, NY, RB, LANES), BF16),
            jax.ShapeDtypeStruct((BLK, WID), F32),
            jax.ShapeDtypeStruct((BLK, WID), F32),
        ),
        in_specs=[in_hbm] * 5,
        out_specs=(in_vmem, in_vmem, in_vmem),
        scratch_shapes=[
            pltpu.VMEM((D, TOK), BF16),
            pltpu.VMEM((TOK, WID), BF16),
            pltpu.VMEM((D, TOK), BF16),
            pltpu.VMEM((BLK, WID), BF16),
            pltpu.VMEM((BLK, WID), BF16),
            pltpu.VMEM((TOK, D), BF16),
            pltpu.VMEM((ROWS, 128), F32),
            pltpu.VMEM((TOK, 128), F32),
            pltpu.VMEM((DP, 128), F32),
            pltpu.VMEM((DP, 128), F32),
            pltpu.VMEM((2, 2 * NZ, ROWS, 128), BF16),
            pltpu.VMEM((TOK, 128), BF16),
            pltpu.VMEM((128, TOK), BF16),
            pltpu.VMEM((TOK // LANES, NX, QUARTERS, NY, RB, LANES), BF16),
            pltpu.VMEM((len(X_FIRST), NX - 1, NY, RB, LANES), BF16),
            pltpu.VMEM((len(X_FIRST), NY, RB, LANES), BF16),
            pltpu.VMEM((len(X_FIRST), NY - 1, RB, LANES), BF16),
            pltpu.VMEM((len(Y_FIRST), NY - 1, NX, RB, LANES), BF16),
            pltpu.VMEM((len(Y_FIRST), NX, RB, LANES), BF16),
            pltpu.VMEM((len(Y_FIRST), NX - 1, RB, LANES), BF16),
            pltpu.VMEM((2, 2, NZ, ROWS, 128), BF16),
            pltpu.VMEM((2, NZ, ROWS, 128), BF16),
            pltpu.VMEM((2, NZ, ROWS, 128), BF16),
            pltpu.VMEM((2, NZ - 1, ROWS, 128), BF16),
            dma((5,)), dma((2, NZ)), dma((2, NZ)), dma((2,)),
            dma((2,)), dma((2,)), dma((2,)), dma((2,)),
            *[dma((len(CHUNKS),)) for _ in range(8)],
        ],
        compiler_params=pltpu.CompilerParams(
            collective_id=0, has_side_effects=True, vmem_limit_bytes=40 << 20
        ),
    )(*operands)
    grad_input, grad_up, grad_down = pl.pallas_call(
        store,
        out_shape=(
            jax.ShapeDtypeStruct((D, TOK), BF16),
            jax.ShapeDtypeStruct((BLK, WID), F32),
            jax.ShapeDtypeStruct((BLK, WID), F32),
        ),
        in_specs=[pl.BlockSpec(memory_space=pl.ANY)] * 3,
        out_specs=(in_hbm,) * 3,
        scratch_shapes=[dma((TOK // LANES + 2,))],
        compiler_params=pltpu.CompilerParams(vmem_limit_bytes=4 << 20),
    )(grad_input.reshape(TOK // LANES, DP, LANES), grad_up, grad_down)
    return grad_input.T, grad_up, grad_down.T


def solution(mesh):
    split = Mesh(mesh.devices.reshape(NZ, NC, NY, NX), AXES)
    fs, tp = ("z", "c"), ("y", "x")
    return jax.shard_map(
        on_device,
        mesh=split,
        in_specs=(P(fs, None), P(fs, tp), P(fs, None), P(fs, tp), P(tp, fs)),
        out_specs=(P(fs, None), P(fs, tp), P(tp, fs)),
        check_vma=False,
    )
```

time: 70.2 us -> 62.6 us (0.89)
  local copies, waits for them, and re-layouts: 5.93 us -> 0 us
  Pallas kernels: 62.2 us -> 60.9 us
    unnamed x12 -> x0, local copies, waits for them, and re-layouts: 5.93 us -> none
    pallas_call x1 -> x2, Pallas kernels: 62.2 us -> 60.9 us  [the longest x1 59.8 us: on_device(): pl.pallas_call(kernel, out_shape=(jax.ShapeDtypeStruct((TOK // LANES, NX,...]
where the time goes in v2:
time: 62.6 us; the launch traced here: 61.5 us
  Pallas kernels  60.9 us (97%)
  between operations  0.64 us (1%)
    pallas_call x1, Pallas kernels, on_device(): pl.pallas_call(kernel, out_shape=(jax.ShapeDtypeStruct((TOK // LANES, NX,...  59.8 us

profile of v2, /device:TPU:1, one launch (start us, length us, event | category | flops | bytes accessed | tf_op | source)
XLA Modules:
  0.0 61.5 jit_solution(7932056251304921663)
XLA Ops:
  0.6 59.8 %shard_map.76 = (bf16[2,4,4,8,16,128]{5,4,3,2,1,0:T(8,128)(2,1)S(1)}, f32[84,126]{1,0:T(8,128)S(1)}, f32[84,126]{1,0:T(8,128)S(1)}) custom-call(bf16[2016,256]{1,0:T(8,128)(2,1)} %bitcast.7, bf16[256,126]{1,0:T(8,128)(2,1)} %pre_hbm.1, bf16[2016,256]{1,0:T(8,128)(2,1)} %bitcast.8, bf16[84,126]{1,0:T(8,128)(2,1)} %wup_hbm.1, bf16[84,126]{1,0:T(8,128)(2,1)} %bitcast.9), custom_call_target="tpu_custom_call" | custom-call | tf_op jit(solution)/shard_map/pallas_call | solution.py:337
  60.5 1.0 %shard_map.77 = (bf16[2016,256]{1,0:T(8,128)(2,1)}, f32[84,126]{1,0:T(8,128)}, f32[84,126]{1,0:T(8,128)}) custom-call(bf16[2,2048,128]{2,1,0:T(8,128)(2,1)S(1)} %bitcast.6, f32[84,126]{1,0:T(8,128)S(1)} %get-tuple-element.10.gup, f32[84,126]{1,0:T(8,128)S(1)} %get-tuple-element.11.gdown), custom_call_target="tpu_custom_call" | custom-call | tf_op jit(solution)/shard_map/pallas_call | solution.py:379

commit v3 on v2

v3 whole, which is shorter than its diff:
```python
import functools

import jax
import jax.numpy as jnp
from jax import lax
from jax.experimental import pallas as pl
from jax.experimental.pallas import tpu as pltpu
from jax.sharding import Mesh
from jax.sharding import PartitionSpec as P

AXES = ("z", "c", "y", "x")
NZ, NC, NY, NX = 12, 2, 8, 4
MESH_IDS = pl.DeviceIdType.MESH
F32 = jnp.float32
BF16 = jnp.bfloat16
TOK, D, WID, BLK = 256, 2016, 126, 84
DP, TILES = 2048, 11
ROWS = 8 * TILES
LANES, QUARTERS, RB = 128, 4, 16
CHUNKS = [(h, q) for h in range(TOK // LANES) for q in range(QUARTERS)]
Y_FIRST = (1,)
X_FIRST = tuple(i for i in range(len(CHUNKS)) if i not in Y_FIRST)
ORDER = tuple(range(len(CHUNKS)))
PER_CHUNK = 2 * (NY - 1 + (NX - 1) * NY) * RB // 8
assert PER_CHUNK == 2 * (NX - 1 + (NY - 1) * NX) * RB // 8
SENT = 2 * TILES * (23 + NZ + NZ - 1) + len(CHUNKS) * PER_CHUNK
X_TIMES = (4.3, 9.0, 13.7)
Y_TIMES = (8.5, 15.0, 18.5)
X_STEP, Y_STEP = 1.4, 3.0


def kernel(
    inputs_hbm, pre_hbm, cot_hbm, wup_hbm, wdown_hbm,
    gi, gup_out, gdown_out,
    inp, pre, cot, wup, wdn,
    cotn, scr, pact, wc, grad, wg, pgrad, pgt, part,
    x_in1, x_sum, y_in2, y_in1, y_sum, x_in2, done, gsum,
    gs, sib, cs, zr,
    sent, ld_sem, ag_recv, ag_sib, sib_recv, z_recv,
    r1, r2, r3, r4, met, own_sem, send_sem,
):
    z, c, y, x = (lax.axis_index(a) for a in AXES)

    def zpeer(d):
        return {"z": lax.rem(z + (d + NZ), NZ)}

    def ypeer(d):
        return {"y": lax.rem(y + d, NY)}

    def xpeer(d):
        return {"x": lax.rem(x + d, NX)}

    other = {"c": 1 - c}

    def send(src, dst, rsem, to):
        pltpu.make_async_remote_copy(
            src_ref=src, dst_ref=dst, send_sem=send_sem, recv_sem=rsem,
            device_id=to, device_id_type=MESH_IDS,
        ).start()

    def wait(ref, sem):
        pltpu.make_async_copy(ref, ref, sem).wait()

    loads = [
        pltpu.make_async_copy(a, b, ld_sem.at[i])
        for i, (a, b) in enumerate(
            ((wdown_hbm, wdn), (wup_hbm, wup), (pre_hbm, pre), (cot_hbm, cot), (inputs_hbm, inp))
        )
    ]
    for copy in loads:
        copy.start()

    barrier = pltpu.get_barrier_semaphore()
    peers = [zpeer(d) for d in (3, -3, 2, -2, 1, -1)] + [other]
    peers += [xpeer(1), xpeer(NX - 1), ypeer(1), ypeer(NY - 1)]
    for to in peers:
        pl.semaphore_signal(barrier, inc=1, device_id=to, device_id_type=MESH_IDS)

    mine = 2 * z + c

    def tiles(block):
        return block.reshape(TILES, 8, 128).astype(BF16)

    scr[...] = jnp.zeros_like(scr)
    loads[0].wait()
    scr[0:BLK, 0:WID] = wdn[...].astype(F32)
    wg[0, mine] = tiles(scr[...])
    loads[1].wait()
    scr[0:BLK, 0:WID] = wup[...].astype(F32)
    wg[1, mine] = tiles(scr[...])

    pl.semaphore_wait(barrier, len(peers))

    def meet(r):
        links = [(met.at[r], ypeer(1)), (met.at[3 + r], ypeer(NY - 1))]
        if r == 0:
            links += [(met.at[6], xpeer(1)), (met.at[7], xpeer(NX - 1))]
        for sem, to in links:
            pl.semaphore_signal(sem, inc=1, device_id=to, device_id_type=MESH_IDS)

    def met_all(r):
        for i in (r, 3 + r, *((6, 7) if r == 0 else ())):
            pl.semaphore_wait(met.at[i], 1)

    meet(0)

    near = jnp.where(lax.rem(z + 3, NZ) < NZ // 2, -1, 1)
    sides = (near, -near)

    def slot(d):
        return lax.rem(d + NZ, NZ)

    def block_from(d):
        return 2 * lax.rem(z - d + NZ, NZ) + c

    def ag_own(w, *steps):
        ref = wg.at[w, mine]
        for d in steps:
            send(ref, ref, ag_recv.at[w, d % NZ], zpeer(d))

    def ag_own_pair(w):
        ref = wg.at[w, mine]
        send(ref, ref, ag_sib.at[w], other)

    def ag_wait(w, d):
        wait(wg.at[w, block_from(d)], ag_recv.at[w, slot(d)])

    def ag_relay(w, side):
        ref = wg.at[w, block_from(3 * side)]

        @pl.when(c == (1 - side) // 2)
        def _():
            send(ref, ref, ag_recv.at[w, 6], zpeer(3 * side))

        ag_step(w, 3 * side, side)

        ag_step(w, 3 * side, 2 * side)

    def ag_step(w, d, step):
        ref = wg.at[w, block_from(d)]
        send(ref, ref, ag_recv.at[w, slot(d + step)], zpeer(step))

    def ag_pass(w, d):
        ref = wg.at[w, block_from(d)]
        send(ref, ref, ag_sib.at[w], other)

    def ag_last(w):
        wait(wg.at[w, pl.ds(0, NZ)], ag_sib.at[w])

    def compact(w):
        for f in range(2 * NZ):
            wc[f * BLK : f * BLK + ROWS, :] = wg[w, f].astype(F32).reshape(ROWS, 128)

    def to_blocks(g):
        for f in range(2 * NZ):
            gs[g, f % 2, f // 2] = tiles(grad[f * BLK : f * BLK + ROWS, :])

    def pair_send(g):
        send(gs.at[g, 1 - c], sib.at[g], sib_recv.at[g], other)

    def pair_sum(g):
        wait(sib.at[g], sib_recv.at[g])
        for k in range(NZ):
            cs[g, k] = (gs[g, c, k].astype(F32) + sib[g, k].astype(F32)).astype(BF16)

    def z_out(g):
        for d in (6, 5, -5, 4, -4, 3, -3, 2, -2, 1, -1):
            to = lax.rem(z + (d + NZ), NZ)
            send(cs.at[g, to], zr.at[g, d % NZ - 1], z_recv.at[g], {"z": to})

    def z_sum(g):
        wait(zr.at[g], z_recv.at[g])
        total = cs[g, z].astype(F32)
        for k in range(NZ - 1):
            total = total + zr[g, k].astype(F32)
        return total

    for w in range(2):
        ag_own(w, 3, -3)
    for w in range(2):
        ag_own_pair(w)
        ag_own(w, 1, -1)

    wc[D:DP, :] = jnp.zeros((DP - D, 128), F32)
    grad[D:DP, :] = jnp.zeros((DP - D, 128), F32)
    pact[...] = jnp.zeros_like(pact)
    loads[2].wait()
    pact[:, 0:WID] = jnp.maximum(pre[...].astype(F32), 0.0)
    positive = pact[...]
    hidden = (positive * positive).astype(BF16)
    loads[3].wait()
    cotn[...] = cot[...].T
    grad[0:D, :] = jnp.dot(cot[...], hidden, preferred_element_type=F32)
    to_blocks(0)
    pair_send(0)

    for w in range(2):
        for side in sides:
            ag_wait(w, 3 * side)
            ag_relay(w, side)
    met_all(0)
    meet(1)
    for w in range(2):
        for side in sides:
            ag_wait(w, side)
            ag_step(w, side, side)
    for w in range(2):
        for side in sides:
            ag_pass(w, 3 * side)
            ag_pass(w, side)
    for w in range(2):
        for side in sides:
            ag_wait(w, 4 * side)
    pair_sum(0)
    met_all(1)
    meet(2)

    def ag_end(w):
        for side in sides:
            ag_pass(w, 4 * side)
        for side in sides:
            ag_wait(w, 2 * side)
            ag_pass(w, 2 * side)
        ag_wait(w, 6)
        ag_pass(w, 6)
        for side in sides:
            ag_wait(w, 5 * side)
            ag_pass(w, 5 * side)

    ag_end(0)
    ag_end(1)
    ag_last(0)
    compact(0)
    hidden_grad = jnp.dot(cotn[...], wc[0:D, :].astype(BF16), preferred_element_type=F32)
    pre_grad = 2.0 * pact[...] * hidden_grad
    pgrad[...] = pre_grad.astype(BF16)
    pgt[...] = pre_grad.T.astype(BF16)
    met_all(2)
    ag_last(1)
    compact(1)

    def others(n):
        return sorted(range(1, n), key=lambda d: -min(d, n - d))

    def scatter(n, me, axis, src, dst, rsem):
        for d in others(n):
            to = lax.rem(me + d, n)
            send(src(to), dst.at[d - 1], rsem, {axis: to})

    def share(n, me, axis, src, dst, rsem):
        for d in others(n):
            send(src, dst, rsem, {axis: lax.rem(me + d, n)})

    def total(own, arrived):
        out = own.astype(F32)
        for j in range(arrived.shape[0]):
            out = out + arrived[j].astype(F32)
        return out.astype(BF16)

    def stage0(i):
        h, q = CHUNKS[i]
        for s in range(NX):
            start = (s * QUARTERS + q) * NY * RB
            rows = wc[start : start + NY * RB, :].astype(BF16)
            half = pgt[:, h * LANES : (h + 1) * LANES]
            product = jnp.dot(rows, half, preferred_element_type=F32).astype(BF16)
            part[h, s, q] = product.reshape(NY, RB, LANES)
        if i in Y_FIRST:
            dst = y_in1.at[Y_FIRST.index(i)]
            scatter(NY, y, "y", lambda to: part.at[h, :, q, to], dst, r1.at[i])
        else:
            dst = x_in1.at[X_FIRST.index(i)]
            scatter(NX, x, "x", lambda to: part.at[h, to, q], dst, r1.at[i])

    def stage1(i):
        h, q = CHUNKS[i]
        if i in Y_FIRST:
            j = Y_FIRST.index(i)
            wait(y_in1.at[j], r1.at[i])
            y_sum[j] = total(part[h, :, q, y], y_in1.at[j])
            scatter(NX, x, "x", lambda to: y_sum.at[j, to], x_in2.at[j], r2.at[i])
        else:
            j = X_FIRST.index(i)
            wait(x_in1.at[j], r1.at[i])
            x_sum[j] = total(part[h, x, q], x_in1.at[j])
            scatter(NY, y, "y", lambda to: x_sum.at[j, to], y_in2.at[j], r2.at[i])

    def stage2(i):
        h, q = CHUNKS[i]
        to = gi.at[h, x, q, y]
        if i in Y_FIRST:
            j = Y_FIRST.index(i)
            wait(x_in2.at[j], r2.at[i])
            done[i] = total(y_sum[j, x], x_in2.at[j])
            share(NX, x, "x", done.at[i], to, r3.at[i])
        else:
            j = X_FIRST.index(i)
            wait(y_in2.at[j], r2.at[i])
            done[i] = total(x_sum[j, y], y_in2.at[j])
            share(NY, y, "y", done.at[i], to, r3.at[i])
        pltpu.make_async_copy(done.at[i], to, own_sem.at[i]).start()

    def stage3(i):
        h, q = CHUNKS[i]
        pltpu.make_async_copy(done.at[i], gi.at[h, x, q, y], own_sem.at[i]).wait()
        if i in Y_FIRST:
            wait(x_in2.at[Y_FIRST.index(i)], r3.at[i])
            part_of_all = gi.at[h, :, q, y]
            share(NY, y, "y", part_of_all, part_of_all, r4.at[i])
        else:
            wait(y_in2.at[X_FIRST.index(i)], r3.at[i])
            part_of_all = gi.at[h, x, q]
            share(NX, x, "x", part_of_all, part_of_all, r4.at[i])

    def finish(i):
        wait(y_in1.at[Y_FIRST.index(i)] if i in Y_FIRST else x_in1.at[X_FIRST.index(i)], r4.at[i])

    for i in ORDER:
        stage0(i)
    z_out(0)

    loads[4].wait()
    grad[0:D, :] = jnp.dot(inp[...], pgrad[...], preferred_element_type=F32)
    to_blocks(1)
    pair_send(1)

    events = []
    for group, times, step in ((X_FIRST, X_TIMES, X_STEP), (Y_FIRST, Y_TIMES, Y_STEP)):
        for n, stage in enumerate((stage1, stage2, stage3)):
            events += [(times[n] + step * j, i, stage) for j, i in enumerate(group)]
    events.sort(key=lambda e: e[:2])
    for t, (_, i, stage) in enumerate(events):
        stage(i)
        if t == 0:
            pair_sum(1)
            z_out(1)
    for g, out in ((0, gdown_out), (1, gup_out)):
        gsum[g] = z_sum(g).reshape(ROWS, 128)[0:BLK, 0:WID]
        pltpu.make_async_copy(gsum.at[g], out, ld_sem.at[g]).start()
    for i in ORDER:
        finish(i)
    for g, out in ((0, gdown_out), (1, gup_out)):
        pltpu.make_async_copy(gsum.at[g], out, ld_sem.at[g]).wait()
    wait(sent, send_sem)


def store(gi, gup, gdown, gi_out, gup_out, gdown_out, sem):
    pairs = [
        (gi.at[h, pl.ds(0, D)], gi_out.at[:, pl.ds(h * LANES, LANES)])
        for h in range(TOK // LANES)
    ]
    pairs += [(gup, gup_out), (gdown, gdown_out)]
    copies = [pltpu.make_async_copy(a, b, sem.at[i]) for i, (a, b) in enumerate(pairs)]
    for copy in copies:
        copy.start()
    for copy in copies:
        copy.wait()


def on_device(inputs, pre_act, cotangent, w_up, w_down):
    in_hbm = pl.BlockSpec(memory_space=pltpu.HBM)
    anywhere = pl.BlockSpec(memory_space=pl.ANY)
    dma = pltpu.SemaphoreType.DMA
    operands = [
        pltpu.with_memory_space_constraint(a, pltpu.HBM)
        for a in (inputs.T, pre_act, cotangent.T, w_up, w_down.T)
    ]
    grad_input, grad_up, grad_down = pl.pallas_call(
        kernel,
        out_shape=(
            jax.ShapeDtypeStruct((TOK // LANES, NX, QUARTERS, NY, RB, LANES), BF16),
            jax.ShapeDtypeStruct((BLK, WID), F32),
            jax.ShapeDtypeStruct((BLK, WID), F32),
        ),
        in_specs=[in_hbm] * 5,
        out_specs=(anywhere,) * 3,
        scratch_shapes=[
            pltpu.VMEM((D, TOK), BF16),
            pltpu.VMEM((TOK, WID), BF16),
            pltpu.VMEM((D, TOK), BF16),
            pltpu.VMEM((BLK, WID), BF16),
            pltpu.VMEM((BLK, WID), BF16),
            pltpu.VMEM((TOK, D), BF16),
            pltpu.VMEM((ROWS, 128), F32),
            pltpu.VMEM((TOK, 128), F32),
            pltpu.VMEM((DP, 128), F32),
            pltpu.VMEM((DP, 128), F32),
            pltpu.VMEM((2, 2 * NZ, TILES, 8, 128), BF16),
            pltpu.VMEM((TOK, 128), BF16),
            pltpu.VMEM((128, TOK), BF16),
            pltpu.VMEM((TOK // LANES, NX, QUARTERS, NY, RB, LANES), BF16),
            pltpu.VMEM((len(X_FIRST), NX - 1, NY, RB, LANES), BF16),
            pltpu.VMEM((len(X_FIRST), NY, RB, LANES), BF16),
            pltpu.VMEM((len(X_FIRST), NY - 1, RB, LANES), BF16),
            pltpu.VMEM((len(Y_FIRST), NY - 1, NX, RB, LANES), BF16),
            pltpu.VMEM((len(Y_FIRST), NX, RB, LANES), BF16),
            pltpu.VMEM((len(Y_FIRST), NX - 1, RB, LANES), BF16),
            pltpu.VMEM((len(CHUNKS), RB, LANES), BF16),
            pltpu.VMEM((2, BLK, WID), F32),
            pltpu.VMEM((2, 2, NZ, TILES, 8, 128), BF16),
            pltpu.VMEM((2, NZ, TILES, 8, 128), BF16),
            pltpu.VMEM((2, NZ, TILES, 8, 128), BF16),
            pltpu.VMEM((2, NZ - 1, TILES, 8, 128), BF16),
            pltpu.VMEM((SENT, 8, 128), BF16),
            dma((5,)), dma((2, NZ)), dma((2,)), dma((2,)), dma((2,)),
            *[dma((len(CHUNKS),)) for _ in range(4)],
            pltpu.SemaphoreType.REGULAR((8,)), dma((len(CHUNKS),)), dma,
        ],
        compiler_params=pltpu.CompilerParams(
            collective_id=0, has_side_effects=True, vmem_limit_bytes=40 << 20
        ),
    )(*operands)
    grad_input, grad_up, grad_down = pl.pallas_call(
        store,
        out_shape=(
            jax.ShapeDtypeStruct((D, TOK), BF16),
            jax.ShapeDtypeStruct((BLK, WID), F32),
            jax.ShapeDtypeStruct((BLK, WID), F32),
        ),
        in_specs=[anywhere] * 3,
        out_specs=(in_hbm,) * 3,
        scratch_shapes=[dma((TOK // LANES + 2,))],
        compiler_params=pltpu.CompilerParams(vmem_limit_bytes=4 << 20),
    )(grad_input.reshape(TOK // LANES, DP, LANES), grad_up, grad_down)
    return grad_input.T, grad_up, grad_down.T


def solution(mesh):
    split = Mesh(mesh.devices.reshape(NZ, NC, NY, NX), AXES)
    fs, tp = ("z", "c"), ("y", "x")
    return jax.shard_map(
        on_device,
        mesh=split,
        in_specs=(P(fs, None), P(fs, tp), P(fs, None), P(fs, tp), P(tp, fs)),
        out_specs=(P(fs, None), P(fs, tp), P(tp, fs)),
        check_vma=False,
    )
```

time: 62.6 us -> 59.4 us (0.949); the launches traced: 61.5 us -> 59.2 us
  Pallas kernels: 60.9 us -> 58.6 us
    pallas_call x1, Pallas kernels: 59.8 us -> 57.6 us  [on_device(): pl.pallas_call(kernel, out_shape=(jax.ShapeDtypeStruct((TOK // LANES, NX,...]
where the time goes in v3:
time: 59.4 us; the launch traced here: 59.2 us
  Pallas kernels  58.6 us (99%)
  between operations  0.64 us (1%)
    pallas_call x1, Pallas kernels, on_device(): pl.pallas_call(kernel, out_shape=(jax.ShapeDtypeStruct((TOK // LANES, NX,...  57.6 us

profile of v3, /device:TPU:1, one launch (start us, length us, event | category | flops | bytes accessed | tf_op | source)
XLA Modules:
  0.0 59.2 jit_solution(4820120450642969950)
XLA Ops:
  0.6 57.6 %shard_map.76 = (bf16[2,4,4,8,16,128]{5,4,3,2,1,0:T(8,128)(2,1)S(1)}, f32[84,126]{1,0:T(8,128)S(1)}, f32[84,126]{1,0:T(8,128)S(1)}) custom-call(bf16[2016,256]{1,0:T(8,128)(2,1)} %bitcast.7, bf16[256,126]{1,0:T(8,128)(2,1)} %pre_hbm.1, bf16[2016,256]{1,0:T(8,128)(2,1)} %bitcast.8, bf16[84,126]{1,0:T(8,128)(2,1)} %wup_hbm.1, bf16[84,126]{1,0:T(8,128)(2,1)} %bitcast.9), custom_call_target="tpu_custom_call" | custom-call | tf_op jit(solution)/shard_map/pallas_call | solution.py:368
  58.2 1.0 %shard_map.77 = (bf16[2016,256]{1,0:T(8,128)(2,1)}, f32[84,126]{1,0:T(8,128)}, f32[84,126]{1,0:T(8,128)}) custom-call(bf16[2,2048,128]{2,1,0:T(8,128)(2,1)S(1)} %bitcast.6, f32[84,126]{1,0:T(8,128)S(1)} %get-tuple-element.10.gup, f32[84,126]{1,0:T(8,128)S(1)} %get-tuple-element.11.gdown), custom_call_target="tpu_custom_call" | custom-call | tf_op jit(solution)/shard_map/pallas_call | solution.py:413

commit v4 on v3

--- a/solution.py
+++ b/solution.py
@@ -24,6 +24,7 @@
 PER_CHUNK = 2 * (NY - 1 + (NX - 1) * NY) * RB // 8
 assert PER_CHUNK == 2 * (NX - 1 + (NY - 1) * NX) * RB // 8
 SENT = 2 * TILES * (23 + NZ + NZ - 1) + len(CHUNKS) * PER_CHUNK
+LAST = (len(X_FIRST) * (NX - 1) * NY + len(Y_FIRST) * (NY - 1) * NX) * RB // 8
 X_TIMES = (4.3, 9.0, 13.7)
 Y_TIMES = (8.5, 15.0, 18.5)
 X_STEP, Y_STEP = 1.4, 3.0
@@ -61,6 +62,12 @@
     def wait(ref, sem):
         pltpu.make_async_copy(ref, ref, sem).wait()
 
+    barrier = pltpu.get_barrier_semaphore()
+    peers = [zpeer(d) for d in (3, -3, 2, -2, 1, -1)] + [other]
+    peers += [xpeer(1), xpeer(NX - 1), ypeer(1), ypeer(NY - 1)]
+    for to in peers:
+        pl.semaphore_signal(barrier, inc=1, device_id=to, device_id_type=MESH_IDS)
+
     loads = [
         pltpu.make_async_copy(a, b, ld_sem.at[i])
         for i, (a, b) in enumerate(
@@ -69,12 +76,6 @@
     ]
     for copy in loads:
         copy.start()
-
-    barrier = pltpu.get_barrier_semaphore()
-    peers = [zpeer(d) for d in (3, -3, 2, -2, 1, -1)] + [other]
-    peers += [xpeer(1), xpeer(NX - 1), ypeer(1), ypeer(NY - 1)]
-    for to in peers:
-        pl.semaphore_signal(barrier, inc=1, device_id=to, device_id_type=MESH_IDS)
 
     mine = 2 * z + c
 
@@ -306,14 +307,11 @@
         if i in Y_FIRST:
             wait(x_in2.at[Y_FIRST.index(i)], r3.at[i])
             part_of_all = gi.at[h, :, q, y]
-            share(NY, y, "y", part_of_all, part_of_all, r4.at[i])
+            share(NY, y, "y", part_of_all, part_of_all, r4)
         else:
             wait(y_in2.at[X_FIRST.index(i)], r3.at[i])
             part_of_all = gi.at[h, x, q]
-            share(NX, x, "x", part_of_all, part_of_all, r4.at[i])
-
-    def finish(i):
-        wait(y_in1.at[Y_FIRST.index(i)] if i in Y_FIRST else x_in1.at[X_FIRST.index(i)], r4.at[i])
+            share(NX, x, "x", part_of_all, part_of_all, r4)
 
     for i in ORDER:
         stage0(i)
@@ -337,10 +335,9 @@
     for g, out in ((0, gdown_out), (1, gup_out)):
         gsum[g] = z_sum(g).reshape(ROWS, 128)[0:BLK, 0:WID]
         pltpu.make_async_copy(gsum.at[g], out, ld_sem.at[g]).start()
-    for i in ORDER:
-        finish(i)
     for g, out in ((0, gdown_out), (1, gup_out)):
         pltpu.make_async_copy(gsum.at[g], out, ld_sem.at[g]).wait()
+    wait(sent.at[pl.ds(0, LAST)], r4)
     wait(sent, send_sem)
 
 
@@ -403,7 +400,7 @@
             pltpu.VMEM((2, NZ - 1, TILES, 8, 128), BF16),
             pltpu.VMEM((SENT, 8, 128), BF16),
             dma((5,)), dma((2, NZ)), dma((2,)), dma((2,)), dma((2,)),
-            *[dma((len(CHUNKS),)) for _ in range(4)],
+            *[dma((len(CHUNKS),)) for _ in range(3)], dma,
             pltpu.SemaphoreType.REGULAR((8,)), dma((len(CHUNKS),)), dma,
         ],
         compiler_params=pltpu.CompilerParams(

time: 59.4 us -> 59.3 us (level)
  no operation moved by 1% of the time
where the time goes in v4:
time: 59.3 us; the launch traced here: 59.2 us
  Pallas kernels  58.5 us (99%)
  between operations  0.64 us (1%)
    pallas_call x1, Pallas kernels, on_device(): pl.pallas_call(kernel, out_shape=(jax.ShapeDtypeStruct((TOK // LANES, NX,...  57.5 us

profile of v4, /device:TPU:1, one launch (start us, length us, event | category | flops | bytes accessed | tf_op | source)
XLA Modules:
  0.0 59.2 jit_solution(13291072028563677226)
XLA Ops:
  0.6 57.5 %shard_map.76 = (bf16[2,4,4,8,16,128]{5,4,3,2,1,0:T(8,128)(2,1)S(1)}, f32[84,126]{1,0:T(8,128)S(1)}, f32[84,126]{1,0:T(8,128)S(1)}) custom-call(bf16[2016,256]{1,0:T(8,128)(2,1)} %bitcast.7, bf16[256,126]{1,0:T(8,128)(2,1)} %pre_hbm.1, bf16[2016,256]{1,0:T(8,128)(2,1)} %bitcast.8, bf16[84,126]{1,0:T(8,128)(2,1)} %wup_hbm.1, bf16[84,126]{1,0:T(8,128)(2,1)} %bitcast.9), custom_call_target="tpu_custom_call" | custom-call | tf_op jit(solution)/shard_map/pallas_call | solution.py:365
  58.2 1.0 %shard_map.77 = (bf16[2016,256]{1,0:T(8,128)(2,1)}, f32[84,126]{1,0:T(8,128)}, f32[84,126]{1,0:T(8,128)}) custom-call(bf16[2,2048,128]{2,1,0:T(8,128)(2,1)S(1)} %bitcast.6, f32[84,126]{1,0:T(8,128)S(1)} %get-tuple-element.10.gup, f32[84,126]{1,0:T(8,128)S(1)} %get-tuple-element.11.gdown), custom_call_target="tpu_custom_call" | custom-call | tf_op jit(solution)/shard_map/pallas_call | solution.py:410

commit v5 on v4

--- a/solution.py
+++ b/solution.py
@@ -38,7 +38,7 @@
     x_in1, x_sum, y_in2, y_in1, y_sum, x_in2, done, gsum,
     gs, sib, cs, zr,
     sent, ld_sem, ag_recv, ag_sib, sib_recv, z_recv,
-    r1, r2, r3, r4, met, own_sem, send_sem,
+    r1, r2, r4, met, send_sem,
 ):
     z, c, y, x = (lax.axis_index(a) for a in AXES)
 
@@ -293,23 +293,23 @@
             j = Y_FIRST.index(i)
             wait(x_in2.at[j], r2.at[i])
             done[i] = total(y_sum[j, x], x_in2.at[j])
-            share(NX, x, "x", done.at[i], to, r3.at[i])
+            share(NX, x, "x", done.at[i], to, r1.at[i])
         else:
             j = X_FIRST.index(i)
             wait(y_in2.at[j], r2.at[i])
             done[i] = total(x_sum[j, y], y_in2.at[j])
-            share(NY, y, "y", done.at[i], to, r3.at[i])
-        pltpu.make_async_copy(done.at[i], to, own_sem.at[i]).start()
+            share(NY, y, "y", done.at[i], to, r1.at[i])
+        pltpu.make_async_copy(done.at[i], to, r2.at[i]).start()
 
     def stage3(i):
         h, q = CHUNKS[i]
-        pltpu.make_async_copy(done.at[i], gi.at[h, x, q, y], own_sem.at[i]).wait()
+        pltpu.make_async_copy(done.at[i], gi.at[h, x, q, y], r2.at[i]).wait()
         if i in Y_FIRST:
-            wait(x_in2.at[Y_FIRST.index(i)], r3.at[i])
+            wait(x_in2.at[Y_FIRST.index(i)], r1.at[i])
             part_of_all = gi.at[h, :, q, y]
             share(NY, y, "y", part_of_all, part_of_all, r4)
         else:
-            wait(y_in2.at[X_FIRST.index(i)], r3.at[i])
+            wait(y_in2.at[X_FIRST.index(i)], r1.at[i])
             part_of_all = gi.at[h, x, q]
             share(NX, x, "x", part_of_all, part_of_all, r4)
 
@@ -400,8 +400,8 @@
             pltpu.VMEM((2, NZ - 1, TILES, 8, 128), BF16),
             pltpu.VMEM((SENT, 8, 128), BF16),
             dma((5,)), dma((2, NZ)), dma((2,)), dma((2,)), dma((2,)),
-            *[dma((len(CHUNKS),)) for _ in range(3)], dma,
-            pltpu.SemaphoreType.REGULAR((8,)), dma((len(CHUNKS),)), dma,
+            *[dma((len(CHUNKS),)) for _ in range(2)], dma,
+            pltpu.SemaphoreType.REGULAR((8,)), dma,
         ],
         compiler_params=pltpu.CompilerParams(
             collective_id=0, has_side_effects=True, vmem_limit_bytes=40 << 20

time: 59.3 us -> 59.2 us (level)
  no operation moved by 1% of the time
where the time goes in v5:
time: 59.2 us; the launch traced here: 59 us
  Pallas kernels  58.4 us (99%)
  between operations  0.64 us (1%)
    pallas_call x1, Pallas kernels, on_device(): pl.pallas_call(kernel, out_shape=(jax.ShapeDtypeStruct((TOK // LANES, NX,...  57.4 us

profile of v5, /device:TPU:1, one launch (start us, length us, event | category | flops | bytes accessed | tf_op | source)
XLA Modules:
  0.0 59.0 jit_solution(17380750531951865214)
XLA Ops:
  0.6 57.4 %shard_map.76 = (bf16[2,4,4,8,16,128]{5,4,3,2,1,0:T(8,128)(2,1)S(1)}, f32[84,126]{1,0:T(8,128)S(1)}, f32[84,126]{1,0:T(8,128)S(1)}) custom-call(bf16[2016,256]{1,0:T(8,128)(2,1)} %bitcast.7, bf16[256,126]{1,0:T(8,128)(2,1)} %pre_hbm.1, bf16[2016,256]{1,0:T(8,128)(2,1)} %bitcast.8, bf16[84,126]{1,0:T(8,128)(2,1)} %wup_hbm.1, bf16[84,126]{1,0:T(8,128)(2,1)} %bitcast.9), custom_call_target="tpu_custom_call" | custom-call | tf_op jit(solution)/shard_map/pallas_call | solution.py:365
  58.0 1.0 %shard_map.77 = (bf16[2016,256]{1,0:T(8,128)(2,1)}, f32[84,126]{1,0:T(8,128)}, f32[84,126]{1,0:T(8,128)}) custom-call(bf16[2,2048,128]{2,1,0:T(8,128)(2,1)S(1)} %bitcast.6, f32[84,126]{1,0:T(8,128)S(1)} %get-tuple-element.10.gup, f32[84,126]{1,0:T(8,128)S(1)} %get-tuple-element.11.gdown), custom_call_target="tpu_custom_call" | custom-call | tf_op jit(solution)/shard_map/pallas_call | solution.py:410
